TPU v7x, 32 devices: a whole 2x2x4 slice. The times are simulated.
32 devices in a mesh: ep: 8 (over z, x), tp: 4 (over y, core).
Axes of the slice: x: 2, y: 2, z: 4, core: 2. Of those that a mesh axis runs over, the one named last changes fastest.
Arguments:
- tokens: bfloat16 [1024, 2048], P('ep'), may hold values from -6 to 6
- cotangent: bfloat16 [1024, 2048], P('ep'), may hold values from -1.5 to 1.5
- routes: int32 [1024, 2], P('ep'), may hold values from 0 to 3, all different within a row; in each aligned block of 128 rows (0 to 127, 128 to 255, ...) at most 96 rows name the same one
- router: bfloat16 [2048, 4], replicated, may hold values from -0.125 to 0.125
- w_gate: bfloat16 [8, 2048, 2048], P('ep', None, 'tp'), may hold values from -0.125 to 0.125
- w_up: bfloat16 [8, 2048, 2048], P('ep', None, 'tp'), may hold values from -0.125 to 0.125
- w_down: bfloat16 [8, 2048, 2048], P('ep', 'tp'), may hold values from -0.09375 to 0.09375
Outputs:
- token_grad: bfloat16 [1024, 2048], P('ep', 'tp')
- gate_grad: float32 [1024, 2], P('ep')
- grad_gate: bfloat16 [8, 2048, 2048], P('ep', None, 'tp')
- grad_up: bfloat16 [8, 2048, 2048], P('ep', None, 'tp')
- grad_down: bfloat16 [8, 2048, 2048], P('ep', 'tp')
- router_grad: float32 [2048, 4], P(('ep', 'tp'))
Inputs may be any that keep to these rules, and one draw needn't show every extreme that they name: `routes`: each row names 2 different experts. In the rows of one index of ep (aligned blocks of 128 rows) no expert is named by more than 96 rows, a bound that some block reaches.
All inputs are finite; a program needn't handle non-finite values.
Results may differ from a plain program's by a relative error of at most 0.018.
Values may be sent and summed in bfloat16 or wider, within the bound.
A program may use at most 64 MiB of HBM per device.

v0:
```python
import jax
import jax.numpy as jnp
from jax import lax
from jax.sharding import PartitionSpec as P

BLOCKS = 2


def build_slots(block_routes, experts, capacity):
    flat_routes = block_routes.reshape(-1)
    labels = jnp.arange(experts, dtype=jnp.int32)
    hit_mask = (flat_routes[None, :] == labels[:, None]).astype(jnp.int32)
    rank_in = jnp.cumsum(hit_mask, axis=1, dtype=jnp.int32) - 1
    slot_ids = jnp.arange(capacity, dtype=jnp.int32)
    assigned = (hit_mask[:, None, :] == 1) & (rank_in[:, None, :] == slot_ids[None, :, None])
    return assigned.astype(jnp.float32)


def gate_pair(tokens, routes, router, experts):
    logits = jnp.dot(tokens, router, preferred_element_type=jnp.float32)
    labels = jnp.arange(experts, dtype=jnp.int32)
    picked = (routes[:, :, None] == labels[None, None, :]).astype(jnp.float32)
    chosen = jnp.sum(picked * logits[:, None, :], axis=2)
    margin = chosen[:, 0] - chosen[:, 1]
    weights = jnp.stack([jax.nn.sigmoid(margin), jax.nn.sigmoid(-margin)], axis=1)
    return (picked, weights)


def logit_grads(picked, weights, gate_grad):
    lead_grad = weights[:, 0] * weights[:, 1] * (gate_grad[:, 0] - gate_grad[:, 1])
    pair_grad = jnp.stack([lead_grad, -lead_grad], axis=1)
    return jnp.sum(picked * pair_grad[:, :, None], axis=1)


def expert_grads(rows_in, cot_in, gate_in, gate_weight, up_weight, down_weight):
    pre_gate = jnp.dot(rows_in, gate_weight, preferred_element_type=jnp.float32)
    pre_up = jnp.dot(rows_in, up_weight, preferred_element_type=jnp.float32)
    back_grad = lax.dot_general(
        cot_in, down_weight, (((1,), (1,)), ((), ())), preferred_element_type=jnp.float32
    )
    sig_gate = jax.nn.sigmoid(pre_gate)
    active = pre_gate * sig_gate
    hidden = (active * pre_up).astype(jnp.bfloat16)
    gate_terms = jnp.sum(hidden.astype(jnp.float32) * back_grad, axis=1)
    gate_col = gate_in.astype(jnp.float32)[:, None]
    scaled_back = gate_col * back_grad
    d_gate = (scaled_back * pre_up * sig_gate * (1.0 + pre_gate * (1.0 - sig_gate))).astype(
        jnp.bfloat16
    )
    d_up = (scaled_back * active).astype(jnp.bfloat16)
    scaled_cot = (gate_col * cot_in.astype(jnp.float32)).astype(jnp.bfloat16)
    contract_rows = (((0,), (0,)), ((), ()))
    grad_gate = lax.dot_general(
        rows_in, d_gate, contract_rows, preferred_element_type=jnp.float32
    ).astype(jnp.bfloat16)
    grad_up = lax.dot_general(
        rows_in, d_up, contract_rows, preferred_element_type=jnp.float32
    ).astype(jnp.bfloat16)
    grad_down = lax.dot_general(
        hidden, scaled_cot, contract_rows, preferred_element_type=jnp.float32
    ).astype(jnp.bfloat16)
    return (d_gate, d_up, gate_terms, grad_gate, grad_up, grad_down)


def spread_slabs(packed, experts, slab_count):
    widened = jnp.broadcast_to(packed[:, None], (experts, BLOCKS) + packed.shape[1:])
    return widened.reshape((slab_count,) + packed.shape[1:])


def routed_shards(tokens, cotangent, routes, router, w_gate, w_up, w_down):
    highest = lax.Precision.HIGHEST
    ep_count = lax.axis_size("ep")
    tp_count = lax.axis_size("tp")
    experts = ep_count // BLOCKS
    tok_rows, width = tokens.shape
    top_count = routes.shape[1]
    capacity = 3 * tok_rows * top_count // (2 * experts)
    col_width = width // tp_count
    tp_index = lax.axis_index("tp")
    picked, weights = gate_pair(tokens, routes, router, experts)
    assigned = build_slots(routes, experts, capacity)
    per_token = jnp.sum(assigned.reshape(experts, capacity, tok_rows, top_count), axis=3)
    token_map = per_token.astype(jnp.bfloat16)
    gate_send = weights.astype(jnp.bfloat16)
    gate_slots = jnp.einsum(
        "ecj,j->ec", assigned, gate_send.astype(jnp.float32).reshape(-1), precision=highest
    ).astype(jnp.bfloat16)
    gate_out = spread_slabs(gate_slots, experts, ep_count)

    def pack_rows(source):
        packed = jnp.einsum(
            "ect,td->ecd", token_map, source, preferred_element_type=jnp.float32
        ).astype(jnp.bfloat16)
        return spread_slabs(packed, experts, ep_count)

    tok_part = lax.dynamic_slice_in_dim(tokens, tp_index * col_width, col_width, 1)
    cot_part = lax.dynamic_slice_in_dim(cotangent, tp_index * col_width, col_width, 1)
    recv_part, recv_cot_part, recv_gate = (
        lax.all_to_all(pack_rows(tok_part), "ep", split_axis=0, concat_axis=0, tiled=True),
        lax.all_to_all(pack_rows(cot_part), "ep", split_axis=0, concat_axis=0, tiled=True),
        lax.all_to_all(gate_out, "ep", split_axis=0, concat_axis=0, tiled=True),
    )
    recv_rows, recv_cot = (
        lax.all_gather(recv_part, "tp", axis=2, tiled=True),
        lax.all_gather(recv_cot_part, "tp", axis=2, tiled=True),
    )
    rows_in = recv_rows.reshape(-1, width)
    cot_in = recv_cot.reshape(-1, width)
    gate_in = recv_gate.reshape(-1)
    d_gate, d_up, gate_terms, grad_gate, grad_up, grad_down = expert_grads(
        rows_in, cot_in, gate_in, w_gate[0], w_up[0], w_down[0]
    )
    contract_hidden = (((1,), (1,)), ((), ()))
    partial_dx = lax.dot_general(
        d_gate, w_gate[0], contract_hidden, preferred_element_type=jnp.float32
    )
    partial_dx = partial_dx + lax.dot_general(
        d_up, w_up[0], contract_hidden, preferred_element_type=jnp.float32
    )
    summed_dx = lax.psum_scatter(
        partial_dx.reshape(ep_count, capacity, width).astype(jnp.bfloat16),
        "tp",
        scatter_dimension=2,
        tiled=True,
    ).astype(jnp.float32)
    gate_sums = lax.psum(gate_terms.reshape(ep_count, capacity), "tp")
    back_dx, back_gate = (
        lax.all_to_all(
            summed_dx.astype(jnp.bfloat16), "ep", split_axis=0, concat_axis=0, tiled=True
        ).astype(summed_dx.dtype),
        lax.all_to_all(
            gate_sums.astype(jnp.bfloat16), "ep", split_axis=0, concat_axis=0, tiled=True
        ).astype(gate_sums.dtype),
    )
    slab_dx = jnp.sum(back_dx.reshape(experts, BLOCKS, capacity, col_width), axis=1)
    routed_dx = jnp.einsum("ect,ecd->td", per_token, slab_dx, precision=highest)
    slab_gate = jnp.sum(back_gate.reshape(experts, BLOCKS, capacity), axis=1)
    gate_grad = jnp.einsum("ecj,ec->j", assigned, slab_gate, precision=highest).reshape(
        tok_rows, top_count
    )
    logit_grad = logit_grads(picked, weights, gate_grad)
    router_cols = lax.dynamic_slice_in_dim(router, tp_index * col_width, col_width, 0).astype(
        jnp.float32
    )
    token_grad = (routed_dx + jnp.dot(logit_grad, router_cols.T, precision=highest)).astype(
        jnp.bfloat16
    )
    seg_rows = tok_rows // tp_count
    own_rows = lax.dynamic_slice_in_dim(tokens, tp_index * seg_rows, seg_rows, 0).astype(
        jnp.float32
    )
    own_logit = lax.dynamic_slice_in_dim(logit_grad, tp_index * seg_rows, seg_rows, 0)
    router_grad = lax.psum_scatter(
        jnp.dot(own_rows.T, own_logit, precision=highest),
        ("ep", "tp"),
        scatter_dimension=0,
        tiled=True,
    )
    return (token_grad, gate_grad, grad_gate[None], grad_up[None], grad_down[None], router_grad)


def gather_rows(part):
    rows = lax.all_gather(part, "ep", axis=0, tiled=True)
    return lax.all_gather(rows, "tp", axis=1, tiled=True)


def scatter_rows(partial):
    by_col = lax.psum_scatter(partial, "tp", scatter_dimension=1, tiled=True)
    return lax.psum_scatter(by_col, "ep", scatter_dimension=0, tiled=True)


def dense_shards(tokens, cotangent, routes, router, w_gate, w_up, w_down):
    highest = lax.Precision.HIGHEST
    ep_count = lax.axis_size("ep")
    tp_count = lax.axis_size("tp")
    experts = ep_count // BLOCKS
    tok_rows, width = tokens.shape
    col_width = width // tp_count
    ep_index = lax.axis_index("ep")
    tp_index = lax.axis_index("tp")
    expert = ep_index // BLOCKS
    w_gate, w_up, w_down = (w_gate[0], w_up[0], w_down[0])
    routes_t = lax.all_gather(routes.T.astype(jnp.float32), "ep", axis=1, tiled=True)
    routes_t = routes_t.astype(jnp.int32)
    tok_part = lax.dynamic_slice_in_dim(tokens, tp_index * col_width, col_width, 1)
    cot_part = lax.dynamic_slice_in_dim(cotangent, tp_index * col_width, col_width, 1)
    tok_all = gather_rows(tok_part)
    cot_all = gather_rows(cot_part)
    logits = lax.dot_general(
        router, tok_all, (((0,), (1,)), ((), ())), preferred_element_type=jnp.float32
    )
    labels = jnp.arange(experts, dtype=jnp.int32)[:, None]
    picked = [(routes_t[k][None, :] == labels).astype(jnp.float32) for k in range(2)]
    chosen = [jnp.sum(p * logits, axis=0) for p in picked]
    margin = chosen[0] - chosen[1]
    weights = [jax.nn.sigmoid(margin), jax.nn.sigmoid(-margin)]
    sent = [w.astype(jnp.bfloat16).astype(jnp.float32) for w in weights]
    mine = [(routes_t[k] == expert).astype(jnp.float32) for k in range(2)]
    gate_col = (mine[0] * sent[0] + mine[1] * sent[1])[:, None]
    pre_gate = jnp.dot(tok_all, w_gate, preferred_element_type=jnp.float32)
    pre_up = jnp.dot(tok_all, w_up, preferred_element_type=jnp.float32)
    back_grad = lax.dot_general(
        cot_all, w_down, (((1,), (1,)), ((), ())), preferred_element_type=jnp.float32
    )
    sig_gate = jax.nn.sigmoid(pre_gate)
    active = pre_gate * sig_gate
    hidden = (active * pre_up).astype(jnp.bfloat16)
    gate_terms = jnp.sum(hidden.astype(jnp.float32) * back_grad, axis=1)
    scaled_back = gate_col * back_grad
    d_gate = (scaled_back * pre_up * sig_gate * (1.0 + pre_gate * (1.0 - sig_gate))).astype(
        jnp.bfloat16
    )
    d_up = (scaled_back * active).astype(jnp.bfloat16)
    scaled_cot = (gate_col * cot_all.astype(jnp.float32)).astype(jnp.bfloat16)
    contract_hidden = (((1,), (1,)), ((), ()))
    partial_dx = lax.dot_general(
        d_gate, w_gate, contract_hidden, preferred_element_type=jnp.float32
    )
    partial_dx = partial_dx + lax.dot_general(
        d_up, w_up, contract_hidden, preferred_element_type=jnp.float32
    )
    routed_dx = scatter_rows(partial_dx.astype(jnp.bfloat16))
    gate_sum = lax.psum(jnp.stack([mine[0] * gate_terms, mine[1] * gate_terms]), ("ep", "tp"))
    contract_rows = (((0,), (0,)), ((), ()))
    grad_gate = lax.dot_general(
        tok_all, d_gate, contract_rows, preferred_element_type=jnp.float32
    ).astype(jnp.bfloat16)
    grad_up = lax.dot_general(
        tok_all, d_up, contract_rows, preferred_element_type=jnp.float32
    ).astype(jnp.bfloat16)
    grad_down = lax.dot_general(
        hidden, scaled_cot, contract_rows, preferred_element_type=jnp.float32
    ).astype(jnp.bfloat16)
    lead = weights[0] * weights[1] * (gate_sum[0] - gate_sum[1])
    logit_grad = (picked[0] - picked[1]) * lead[None, :]
    own_logit = lax.dynamic_slice_in_dim(logit_grad, ep_index * tok_rows, tok_rows, 1)
    gate_grad = lax.dynamic_slice_in_dim(gate_sum, ep_index * tok_rows, tok_rows, 1).T
    router_cols = lax.dynamic_slice_in_dim(router, tp_index * col_width, col_width, 0)
    token_grad = (
        routed_dx.astype(jnp.float32)
        + lax.dot_general(
            own_logit, router_cols.astype(jnp.float32), (((0,), (1,)), ((), ())), precision=highest
        )
    ).astype(jnp.bfloat16)
    seg = width // (ep_count * tp_count)
    own_cols = lax.dynamic_slice_in_dim(
        tok_all, (ep_index * tp_count + tp_index) * seg, seg, 1
    ).astype(jnp.float32)
    router_grad = lax.dot_general(
        logit_grad, own_cols, (((1,), (0,)), ((), ())), precision=highest
    ).T
    return (token_grad, gate_grad, grad_gate[None], grad_up[None], grad_down[None], router_grad)


def shards(tokens, cotangent, routes, router, w_gate, w_up, w_down):
    slots = 3 * routes.shape[1] * BLOCKS
    dense = slots >= lax.axis_size("ep")
    path = dense_shards if dense else routed_shards
    return path(tokens, cotangent, routes, router, w_gate, w_up, w_down)


def solution(mesh):
    placed = (
        P("ep", None),
        P("ep", None),
        P("ep", None),
        P(),
        P("ep", None, "tp"),
        P("ep", None, "tp"),
        P("ep", "tp", None),
    )
    return jax.shard_map(
        shards,
        mesh=mesh,
        in_specs=placed,
        out_specs=(
            P("ep", "tp"),
            P("ep", None),
            P("ep", None, "tp"),
            P("ep", None, "tp"),
            P("ep", "tp", None),
            P(("ep", "tp"), None),
        ),
        check_vma=False,
    )
```

profile of v0, /device:TPU:0, one launch (start us, length us, event | category | flops | bytes accessed | tf_op | source)
XLA Modules:
  0.0 303.0 jit_solution(7012524095717071216)
XLA Ops:
  7.3 1.7 constant_dynamic-slice_fusion.2
  9.0 0.0 all-gather.9.cloned.1.call-start
  9.0 1.6 constant_dynamic-slice_fusion.1
  10.7 43.1 %all-gather.5.cloned.1.call-done = bf16[1024,512]{1,0:T(8,128)(2,1)} async-done(((bf16[128,512]{1,0:T(8,128)(2,1)}), bf16[1024,512]{1,0:T(8,128)(2,1)}) %all-gather.5.cloned.1.call-update) | async-done | bytes 1048592 | tf_op jit(solution)/shard_map/all_gather | solution.py:163
  53.8 41.6 %all-gather.9.cloned.1.call-done = bf16[1024,512]{1,0:T(8,128)(2,1)} async-done(((bf16[128,512]{1,0:T(8,128)(2,1)}), bf16[1024,512]{1,0:T(8,128)(2,1)}) %all-gather.9.cloned.1.call-update) | async-done | bytes 1048592 | tf_op jit(solution)/shard_map/all_gather | solution.py:163
  95.6 18.3 %all_gather.15 = f32[2,1024]{1,0:T(2,128)S(1)} all-gather(f32[2,128]{1,0:T(2,128)S(1)} %convert_bitcast_fusion), channel_id=1, replica_groups=mesh['ep'=8,'tp'=4] {'ep'}, dimensions={1}, use_global_device_ids=true | all-gather | bytes 9216 | tf_op jit(solution)/shard_map/all_gather | solution.py:183
  113.9 16.3 %all-gather.7.cloned.1.call-done = bf16[1024,2048]{1,0:T(8,128)(2,1)} async-done(((bf16[1024,512]{1,0:T(8,128)(2,1)}), bf16[1024,2048]{1,0:T(8,128)(2,1)}) %all-gather.7.cloned.1.call-update) | async-done | bytes 4194320 | tf_op jit(solution)/shard_map/all_gather | solution.py:164
  130.2 3.5 %select_reduce_fusion = (f32[1024]{0:T(1024)S(1)}, f32[1024]{0:T(1024)S(1)}) fusion(s32[1024]{0:T(1024)S(1)} %bitcast.48, s32[1024]{0:T(1024)S(1)} %bitcast.44, bf16[1024,2048]{1,0:T(8,128)(2,1)} %all-gather.7.cloned.1.call-done, bf16[2048,4]{0,1:T(4,128)(2,1)S(1)} %copy-done.3), kind=kOutput, calls=%fused_computation.31 | convolution fusion | flops 16799744 | bytes 4227072 | tf_op jit(solution)/shard_map/dot_general | solution.py:189
  133.8 3.8 %fusion.8 = f32[1024,512]{0,1:T(8,128)} fusion(bf16[1024,2048]{1,0:T(8,128)(2,1)S(1)} %copy-done.1, bf16[1,2048,512]{2,1,0:T(8,128)(2,1)S(1)} %copy-done), kind=kOutput, calls=%fused_computation.12 | convolution fusion | flops 2147483648 | bytes 8388608 | tf_op jit(solution)/shard_map/dot_general | solution.py:200
  137.6 3.8 %fusion.11 = f32[1024,512]{0,1:T(8,128)} fusion(bf16[1024,2048]{1,0:T(8,128)(2,1)S(1)} %copy-done.1, bf16[1,2048,512]{2,1,0:T(8,128)(2,1)S(1)} %copy-done.6), kind=kOutput, calls=%fused_computation.15 | convolution fusion | flops 2147483648 | bytes 8388608 | tf_op jit(solution)/shard_map/dot_general | solution.py:201
  141.4 24.8 %all-gather.11.cloned.1.call-done = bf16[1024,2048]{1,0:T(8,128)(2,1)} async-done(((bf16[1024,512]{1,0:T(8,128)(2,1)}), bf16[1024,2048]{1,0:T(8,128)(2,1)}) %all-gather.11.cloned.1.call-update) | async-done | bytes 4194320 | tf_op jit(solution)/shard_map/all_gather | solution.py:164
  166.1 8.3 %multiply_reduce_fusion = (f32[1024]{0:T(1024)S(1)}, bf16[1024,512]{0,1:T(8,128)(2,1)}, bf16[1024,512]{0,1:T(8,128)(2,1)S(1)}, bf16[1024,512]{0,1:T(8,128)(2,1)S(1)}) fusion(f32[1024,512]{0,1:T(8,128)} %fusion.11, f32[1024,512]{0,1:T(8,128)} %fusion.8, f32[1024]{0:T(1024)S(1)} %get-tuple-element.15, bf16[1024,2048]{1,0:T(8,128)(2,1)} %all-gather.11.cloned.1.call-done, ...), kind=kOutput, calls=%fused_computation.19 | convolution fusion | flops 2157444096 | bytes 13639680 | tf_op jit(solution)/shard_map/dot_general | solution.py:202
  174.5 2.4 fusion.6
  176.9 4.6 %add_convert_fusion = bf16[1024,2048]{1,0:T(8,128)(2,1)} fusion(f32[1024,2048]{1,0:T(8,128)S(1)} %fusion.6, bf16[1024,512]{0,1:T(8,128)(2,1)S(1)} %get-tuple-element.11, bf16[1,2048,512]{2,1,0:T(8,128)(2,1)S(1)} %copy-done.7), kind=kOutput, calls=%fused_computation.1 | convolution fusion | flops 2151677952 | bytes 15728640 | tf_op jit(solution)/shard_map/dot_general | solution.py:219
  181.5 0.0 reduce-scatter.5.cloned.1.call-start
  181.6 39.9 %psum.7 = f32[2,1024]{1,0:T(2,128)S(1)} all-reduce(f32[2,1024]{1,0:T(2,128)S(1)} %pad_maximum_fusion), channel_id=1, replica_groups=mesh['ep'=8,'tp'=4] {'ep','tp'}, use_global_device_ids=true, to_apply=%region_5.6 | all-reduce | flops 2048 | bytes 16384 | tf_op jit(solution)/shard_map/psum | solution.py:223
  221.5 1.9 fusion.17
  223.4 3.4 %reduce-scatter.3.cloned.1.call-done = bf16[1024,512]{1,0:T(8,128)(2,1)} async-done(((bf16[1024,2048]{1,0:T(8,128)(2,1)}), bf16[1024,512]{1,0:T(8,128)(2,1)}) %reduce-scatter.3.cloned.1.call-update) | async-done | bytes 1048592 | tf_op jit(solution)/shard_map/reduce_scatter | solution.py:168
  226.8 0.6 fusion.24
  227.4 6.4 %fusion.4 = bf16[1,2048,512]{2,1,0:T(8,128)(2,1)} fusion(bf16[1024,2048]{1,0:T(8,128)(2,1)} %all-gather.7.cloned.1.call-done, bf16[1024,512]{0,1:T(8,128)(2,1)} %copy-done.8), kind=kOutput, calls=%fused_computation.8 | convolution fusion | flops 2148532224 | bytes 7340032 | tf_op jit(solution)/shard_map/dot_general | solution.py:225
  233.8 3.7 %fusion.5 = bf16[1,2048,512]{2,1,0:T(8,128)(2,1)} fusion(bf16[1024,2048]{1,0:T(8,128)(2,1)S(1)} %copy-done.2, bf16[1024,512]{0,1:T(8,128)(2,1)S(1)} %get-tuple-element.11), kind=kOutput, calls=%fused_computation.9 | convolution fusion | flops 2148532224 | bytes 7340032 | tf_op jit(solution)/shard_map/dot_general | solution.py:228
  237.5 3.8 %fusion.3 = bf16[1,512,2048]{2,1,0:T(8,128)(2,1)} fusion(bf16[1024,512]{0,1:T(8,128)(2,1)S(1)} %copy-done.9, bf16[1024,2048]{1,0:T(8,128)(2,1)S(1)} %copy-done.5, f32[1024]{0:T(1024)S(1)} %get-tuple-element.15), kind=kOutput, calls=%fused_computation.7 | convolution fusion | flops 2154823680 | bytes 7344128 | tf_op jit(solution)/shard_map/dot_general | solution.py:231
  241.2 53.0 %reduce-scatter.5.cloned.1.call-done = bf16[128,512]{1,0:T(8,128)(2,1)} async-done(((bf16[1024,512]{1,0:T(8,128)(2,1)}), bf16[128,512]{1,0:T(8,128)(2,1)}) %reduce-scatter.5.cloned.1.call-update) | async-done | bytes 131088 | tf_op jit(solution)/shard_map/reduce_scatter | solution.py:169
  294.2 1.9 fusion.16
  (38 shorter events, 0.4 us)
Async XLA Ops:
  7.2 126.6 %copy-start = (bf16[1,2048,512]{2,1,0:T(8,128)(2,1)S(1)}, bf16[1,2048,512]{2,1,0:T(8,128)(2,1)}, u32[]{:S(2)}) copy-start(bf16[1,2048,512]{2,1,0:T(8,128)(2,1)} %param.11) | copy-start | bytes 6291460
  7.2 88.4 %copy-start.4 = (s32[128,2]{0,1:T(2,128)S(1)}, s32[128,2]{0,1:T(2,128)}, u32[]{:S(2)}) copy-start(s32[128,2]{0,1:T(2,128)} %param.9) | copy-start | bytes 3076
  7.2 123.0 %copy-start.3 = (bf16[2048,4]{0,1:T(4,128)(2,1)S(1)}, bf16[2048,4]{0,1:T(4,128)(2,1)}, u32[]{:S(2)}) copy-start(bf16[2048,4]{0,1:T(4,128)(2,1)} %param.10) | copy-start | bytes 49156
  7.2 46.5 %all-gather.5.cloned.1.call-start = ((), (), s32[]{:S(2)}) async-start(), calls=%async_computation.2 | async-start | bytes 1179648 | tf_op jit(solution)/shard_map/all_gather | solution.py:163
  9.0 86.5 %all-gather.9.cloned.1.call-start = ((), (), s32[]{:S(2)}) async-start(), calls=%async_computation.4 | async-start | bytes 1179648 | tf_op jit(solution)/shard_map/all_gather | solution.py:163
  10.6 119.6 %all-gather.7.cloned.1.call-start = ((), (), s32[]{:S(2)}) async-start(), calls=%async_computation.3 | async-start | bytes 5242880 | tf_op jit(solution)/shard_map/all_gather | solution.py:164
  53.8 112.4 %all-gather.11.cloned.1.call-start = ((), (), s32[]{:S(2)}) async-start(), calls=%async_computation.5 | async-start | bytes 5242880 | tf_op jit(solution)/shard_map/all_gather | solution.py:164
  95.5 131.3 %reduce-scatter.3.cloned.1.call-start = ((), (), s32[]{:S(2)}) async-start(), calls=%async_computation.6 | async-start | bytes 5242880 | tf_op jit(solution)/shard_map/reduce_scatter | solution.py:168
  130.2 3.6 %copy-start.1 = (bf16[1024,2048]{1,0:T(8,128)(2,1)S(1)}, bf16[1024,2048]{1,0:T(8,128)(2,1)}, u32[]{:S(2)}) copy-start(bf16[1024,2048]{1,0:T(8,128)(2,1)} %all-gather.7.cloned.1.call-done) | copy-start | bytes 12582916
  133.8 3.8 %copy-start.6 = (bf16[1,2048,512]{2,1,0:T(8,128)(2,1)S(1)}, bf16[1,2048,512]{2,1,0:T(8,128)(2,1)}, u32[]{:S(2)}) copy-start(bf16[1,2048,512]{2,1,0:T(8,128)(2,1)} %param.12) | copy-start | bytes 6291460
  174.5 2.4 copy-start.8
  174.5 2.4 copy-start.7
  181.5 112.8 %reduce-scatter.5.cloned.1.call-start = ((), (), s32[]{:S(2)}) async-start(), calls=%async_computation.7 | async-start | bytes 1179648 | tf_op jit(solution)/shard_map/reduce_scatter | solution.py:169
  227.4 6.4 %copy-start.2 = (bf16[1024,2048]{1,0:T(8,128)(2,1)S(1)}, bf16[1024,2048]{1,0:T(8,128)(2,1)}, u32[]{:S(2)}) copy-start(bf16[1024,2048]{1,0:T(8,128)(2,1)} %all-gather.7.cloned.1.call-done) | copy-start | bytes 12582916
  233.7 3.7 %copy-start.5 = (bf16[1024,2048]{1,0:T(8,128)(2,1)S(1)}, bf16[1024,2048]{1,0:T(8,128)(2,1)}, u32[]{:S(2)}) copy-start(bf16[1024,2048]{1,0:T(8,128)(2,1)} %all-gather.11.cloned.1.call-done) | copy-start | bytes 12582916
  233.7 3.7 %copy-start.9 = (bf16[1024,512]{0,1:T(8,128)(2,1)S(1)}, bf16[1024,512]{0,1:T(8,128)(2,1)}, u32[]{:S(2)}) copy-start(bf16[1024,512]{0,1:T(8,128)(2,1)} %get-tuple-element.9) | copy-start | bytes 3145732
Sparse Core Ops, SparseCore 0:
  10.7 42.9 all-gather.4
  56.4 38.9 all-gather.8
  97.0 33.1 all-gather.6
  131.6 34.4 all-gather.10
  181.6 45.1 reduce-scatter.2
  230.0 64.1 reduce-scatter.4
where the time goes:
time: 303 us
  waiting for transfers between devices  182 us (60%)
  blocking collectives  58.3 us (19%)
  matrix products  43.9 us (14%)
  between operations  14.3 us (5%)
  local copies, waits for them, and re-layouts  3.91 us (1%)
    all_gather x2, waiting for transfers between devices, gather_rows(): rows = lax.all_gather(part, 'ep', axis=0, tiled=True)  84.7 us
    reduce_scatter x1, waiting for transfers between devices, scatter_rows(): return lax.psum_scatter(by_col, 'ep', scatter_dimension=0, tiled=True)  53 us
    all_gather x2, waiting for transfers between devices, gather_rows(): return lax.all_gather(rows, 'tp', axis=1, tiled=True)  41.1 us
    psum x1, blocking collectives, dense_shards(): lax.psum(jnp.stack([mine[0] * gate_terms, mine[1] * gate_terms]), ('ep',...  39.9 us
    all_gather x1, blocking collectives, dense_shards(): lax.all_gather(routes.T.astype(jnp.float32), 'ep', axis=1, tiled=True)  18.3 us
    dot_general x1, matrix products, dense_shards(): lax.dot_general(cot_all, w_down, (((1,), (1,)), ((), ())), preferred_elem...  8.32 us
    dot_general x1, matrix products, dense_shards(): lax.dot_general(tok_all, d_gate, contract_rows, preferred_element_type=jn...  6.36 us
  transfers between devices with their start and end apart: 6, of which 6 were waited for; matrix products, arithmetic and copies ran while one was open for 10% of the time, Pallas kernels for 0%

commit v1 on v0

--- a/solution.py
+++ b/solution.py
@@ -160,7 +160,12 @@
 
 
 def gather_rows(part):
-    rows = lax.all_gather(part, "ep", axis=0, tiled=True)
+    ring = [part]
+    for hop in range(7):
+        ring.append(lax.ppermute(ring[-1], "ep", [(dev, (dev + 1) % 8) for dev in range(8)]))
+    rows = jnp.roll(
+        jnp.concatenate(ring[::-1], axis=0), (lax.axis_index("ep") + 1) * ring[0].shape[0], axis=0
+    )
     return lax.all_gather(rows, "tp", axis=1, tiled=True)
 
 

time: 303 us -> 297 us (0.980)
  waiting for transfers between devices: 182 us -> 170 us
  other arithmetic: 0.07 us -> 5.69 us
  starting transfers between devices: 0.24 us -> 3.27 us
    ppermute x0 -> x14, waiting for transfers between devices: none -> 109 us  [gather_rows(): lax.ppermute(ring[-1], 'ep', [(dev, (dev + 1) % 8) for dev in range(8)])]
    all_gather x2 -> x0, waiting for transfers between devices: 84.7 us -> none  [gather_rows(): rows = lax.all_gather(part, 'ep', axis=0, tiled=True)]
    all_gather x2, waiting for transfers between devices: 41.1 us -> 4.53 us  [gather_rows(): return lax.all_gather(rows, 'tp', axis=1, tiled=True)]
    concatenate x0 -> x2, other arithmetic: none -> 5.62 us  [gather_rows(): jnp.roll(jnp.concatenate(ring[::-1], axis=0), (lax.axis_index('ep') + 1)...]
    ppermute x0 -> x14, starting transfers between devices: none -> 3.11 us  [gather_rows(): lax.ppermute(ring[-1], 'ep', [(dev, (dev + 1) % 8) for dev in range(8)])]
  transfers between devices with their start and end apart: 6 -> 18, of which waited for: 6 -> 17; matrix products, arithmetic and copies ran while one was open for 10% -> 10% of each run, Pallas kernels for 0% -> 0%
where the time goes in v1:
time: 297 us; the launch traced here: 296 us
  waiting for transfers between devices  170 us (57%)
  blocking collectives  56.4 us (19%)
  matrix products  44 us (15%)
  between operations  14.1 us (5%)
  other arithmetic  5.69 us (2%)
  starting transfers between devices  3.27 us (1%)
    ppermute x14, waiting for transfers between devices, gather_rows(): lax.ppermute(ring[-1], 'ep', [(dev, (dev + 1) % 8) for dev in range(8)])  109 us
    reduce_scatter x1, waiting for transfers between devices, scatter_rows(): return lax.psum_scatter(by_col, 'ep', scatter_dimension=0, tiled=True)  53 us
    psum x1, blocking collectives, dense_shards(): lax.psum(jnp.stack([mine[0] * gate_terms, mine[1] * gate_terms]), ('ep',...  39.9 us
    all_gather x1, blocking collectives, dense_shards(): lax.all_gather(routes.T.astype(jnp.float32), 'ep', axis=1, tiled=True)  16.5 us
    dot_general x1, matrix products, dense_shards(): lax.dot_general(cot_all, w_down, (((1,), (1,)), ((), ())), preferred_elem...  8.31 us
    dot_general x1, matrix products, dense_shards(): lax.dot_general(tok_all, d_gate, contract_rows, preferred_element_type=jn...  6.36 us
  transfers between devices with their start and end apart: 18, of which 17 were waited for; matrix products, arithmetic and copies ran while one was open for 10% of the time, Pallas kernels for 0%

profile of v1, /device:TPU:0, one launch (start us, length us, event | category | flops | bytes accessed | tf_op | source)
XLA Modules:
  0.0 296.4 jit_solution(546158714633920526)
XLA Ops:
  11.3 6.5 %collective-permute-done = bf16[128,512]{1,0:T(8,128)(2,1)S(1)} collective-permute-done((bf16[128,512]{1,0:T(8,128)(2,1)S(1)}, bf16[128,512]{1,0:T(8,128)(2,1)S(1)}, u32[]{:S(2)}, u32[]{:S(2)}) %collective-permute-start) | collective-permute-done | bytes 131104 | tf_op jit(solution)/shard_map/ppermute | solution.py:165
  17.8 7.7 %collective-permute-done.1 = bf16[128,512]{1,0:T(8,128)(2,1)S(1)} collective-permute-done((bf16[128,512]{1,0:T(8,128)(2,1)S(1)}, bf16[128,512]{1,0:T(8,128)(2,1)S(1)}, u32[]{:S(2)}, u32[]{:S(2)}) %collective-permute-start.1) | collective-permute-done | bytes 131104 | tf_op jit(solution)/shard_map/ppermute | solution.py:165
  25.5 7.7 %collective-permute-done.2 = bf16[128,512]{1,0:T(8,128)(2,1)S(1)} collective-permute-done((bf16[128,512]{1,0:T(8,128)(2,1)S(1)}, bf16[128,512]{1,0:T(8,128)(2,1)S(1)}, u32[]{:S(2)}, u32[]{:S(2)}) %collective-permute-start.2) | collective-permute-done | bytes 131104 | tf_op jit(solution)/shard_map/ppermute | solution.py:165
  33.2 7.7 %collective-permute-done.3 = bf16[128,512]{1,0:T(8,128)(2,1)S(1)} collective-permute-done((bf16[128,512]{1,0:T(8,128)(2,1)S(1)}, bf16[128,512]{1,0:T(8,128)(2,1)S(1)}, u32[]{:S(2)}, u32[]{:S(2)}) %collective-permute-start.3) | collective-permute-done | bytes 131104 | tf_op jit(solution)/shard_map/ppermute | solution.py:165
  40.8 7.7 %collective-permute-done.4 = bf16[128,512]{1,0:T(8,128)(2,1)S(1)} collective-permute-done((bf16[128,512]{1,0:T(8,128)(2,1)S(1)}, bf16[128,512]{1,0:T(8,128)(2,1)S(1)}, u32[]{:S(2)}, u32[]{:S(2)}) %collective-permute-start.4) | collective-permute-done | bytes 131104 | tf_op jit(solution)/shard_map/ppermute | solution.py:165
  48.6 8.9 %collective-permute-done.5 = bf16[128,512]{1,0:T(8,128)(2,1)S(1)} collective-permute-done((bf16[128,512]{1,0:T(8,128)(2,1)S(1)}, bf16[128,512]{1,0:T(8,128)(2,1)S(1)}, u32[]{:S(2)}, u32[]{:S(2)}) %collective-permute-start.5) | collective-permute-done | bytes 131104 | tf_op jit(solution)/shard_map/ppermute | solution.py:165
  57.4 7.7 %collective-permute-done.6 = bf16[128,512]{1,0:T(8,128)(2,1)S(1)} collective-permute-done((bf16[128,512]{1,0:T(8,128)(2,1)S(1)}, bf16[128,512]{1,0:T(8,128)(2,1)S(1)}, u32[]{:S(2)}, u32[]{:S(2)}) %collective-permute-start.6) | collective-permute-done | bytes 131104 | tf_op jit(solution)/shard_map/ppermute | solution.py:165
  69.2 7.7 %collective-permute-done.7 = bf16[128,512]{1,0:T(8,128)(2,1)S(1)} collective-permute-done((bf16[128,512]{1,0:T(8,128)(2,1)S(1)}, bf16[128,512]{1,0:T(8,128)(2,1)S(1)}, u32[]{:S(2)}, u32[]{:S(2)}) %collective-permute-start.7) | collective-permute-done | bytes 131104 | tf_op jit(solution)/shard_map/ppermute | solution.py:165
  76.8 7.7 %collective-permute-done.8 = bf16[128,512]{1,0:T(8,128)(2,1)S(1)} collective-permute-done((bf16[128,512]{1,0:T(8,128)(2,1)S(1)}, bf16[128,512]{1,0:T(8,128)(2,1)S(1)}, u32[]{:S(2)}, u32[]{:S(2)}) %collective-permute-start.8) | collective-permute-done | bytes 131104 | tf_op jit(solution)/shard_map/ppermute | solution.py:165
  84.5 7.7 %collective-permute-done.9 = bf16[128,512]{1,0:T(8,128)(2,1)S(1)} collective-permute-done((bf16[128,512]{1,0:T(8,128)(2,1)S(1)}, bf16[128,512]{1,0:T(8,128)(2,1)S(1)}, u32[]{:S(2)}, u32[]{:S(2)}) %collective-permute-start.9) | collective-permute-done | bytes 131104 | tf_op jit(solution)/shard_map/ppermute | solution.py:165
  92.2 8.0 %collective-permute-done.10 = bf16[128,512]{1,0:T(8,128)(2,1)S(1)} collective-permute-done((bf16[128,512]{1,0:T(8,128)(2,1)S(1)}, bf16[128,512]{1,0:T(8,128)(2,1)S(1)}, u32[]{:S(2)}, u32[]{:S(2)}) %collective-permute-start.10) | collective-permute-done | bytes 131104 | tf_op jit(solution)/shard_map/ppermute | solution.py:165
  100.2 9.0 %collective-permute-done.11 = bf16[128,512]{1,0:T(8,128)(2,1)S(1)} collective-permute-done((bf16[128,512]{1,0:T(8,128)(2,1)S(1)}, bf16[128,512]{1,0:T(8,128)(2,1)S(1)}, u32[]{:S(2)}, u32[]{:S(2)}) %collective-permute-start.11) | collective-permute-done | bytes 131104 | tf_op jit(solution)/shard_map/ppermute | solution.py:165
  109.1 7.7 %collective-permute-done.12 = bf16[128,512]{1,0:T(8,128)(2,1)S(1)} collective-permute-done((bf16[128,512]{1,0:T(8,128)(2,1)S(1)}, bf16[128,512]{1,0:T(8,128)(2,1)S(1)}, u32[]{:S(2)}, u32[]{:S(2)}) %collective-permute-start.12) | collective-permute-done | bytes 131104 | tf_op jit(solution)/shard_map/ppermute | solution.py:165
  116.8 7.7 %collective-permute-done.13 = bf16[128,512]{1,0:T(8,128)(2,1)S(1)} collective-permute-done((bf16[128,512]{1,0:T(8,128)(2,1)S(1)}, bf16[128,512]{1,0:T(8,128)(2,1)S(1)}, u32[]{:S(2)}, u32[]{:S(2)}) %collective-permute-start.13) | collective-permute-done | bytes 131104 | tf_op jit(solution)/shard_map/ppermute | solution.py:165
  127.6 16.5 %all_gather.9 = f32[2,1024]{1,0:T(2,128)S(1)} all-gather(f32[2,128]{1,0:T(2,128)S(1)} %convert_bitcast_fusion), channel_id=1, replica_groups=mesh['ep'=8,'tp'=4] {'ep'}, dimensions={1}, use_global_device_ids=true | all-gather | bytes 9216 | tf_op jit(solution)/shard_map/all_gather | solution.py:188
  147.8 3.8 %fusion.8 = f32[1024,512]{0,1:T(8,128)} fusion(bf16[1024,2048]{1,0:T(8,128)(2,1)S(1)} %copy-done.1, bf16[1,2048,512]{2,1,0:T(8,128)(2,1)S(1)} %copy-done), kind=kOutput, calls=%fused_computation.16 | convolution fusion | flops 2147483648 | bytes 8388608 | tf_op jit(solution)/shard_map/dot_general | solution.py:205
  151.5 3.8 %fusion.11 = f32[1024,512]{0,1:T(8,128)} fusion(bf16[1024,2048]{1,0:T(8,128)(2,1)S(1)} %copy-done.1, bf16[1,2048,512]{2,1,0:T(8,128)(2,1)S(1)} %copy-done.7), kind=kOutput, calls=%fused_computation.19 | convolution fusion | flops 2147483648 | bytes 8388608 | tf_op jit(solution)/shard_map/dot_general | solution.py:206
  155.3 4.5 %all-gather.5.cloned.1.call-done = bf16[1024,2048]{1,0:T(8,128)(2,1)} async-done(((bf16[1024,512]{1,0:T(8,128)(2,1)}), bf16[1024,2048]{1,0:T(8,128)(2,1)}) %all-gather.5.cloned.1.call-update) | async-done | bytes 4194320 | tf_op jit(solution)/shard_map/all_gather | solution.py:169
  159.8 8.3 %multiply_reduce_fusion = (f32[1024]{0:T(1024)S(1)}, bf16[1024,512]{0,1:T(8,128)(2,1)}, bf16[1024,512]{0,1:T(8,128)(2,1)S(1)}, bf16[1024,512]{0,1:T(8,128)(2,1)S(1)}) fusion(f32[1024,512]{0,1:T(8,128)} %fusion.11, f32[1024,512]{0,1:T(8,128)} %fusion.8, f32[1024]{0:T(1024)S(1)} %get-tuple-element.16, bf16[1024,2048]{1,0:T(8,128)(2,1)} %all-gather.5.cloned.1.call-done, ...), kind=kOutput, calls=%fused_computation.23 | convolution fusion | flops 2157444096 | bytes 13639680 | tf_op jit(solution)/shard_map/dot_general | solution.py:207
  170.5 4.6 %add_convert_fusion = bf16[1024,2048]{1,0:T(8,128)(2,1)} fusion(f32[1024,2048]{1,0:T(8,128)S(1)} %fusion.6, bf16[1024,512]{0,1:T(8,128)(2,1)S(1)} %get-tuple-element.12, bf16[1,2048,512]{2,1,0:T(8,128)(2,1)S(1)} %copy-done.8), kind=kOutput, calls=%fused_computation.1 | convolution fusion | flops 2151677952 | bytes 15728640 | tf_op jit(solution)/shard_map/dot_general | solution.py:224
  175.3 39.9 %psum.7 = f32[2,1024]{1,0:T(2,128)S(1)} all-reduce(f32[2,1024]{1,0:T(2,128)S(1)} %pad_maximum_fusion), channel_id=1, replica_groups=mesh['ep'=8,'tp'=4] {'ep','tp'}, use_global_device_ids=true, to_apply=%region_5.7 | all-reduce | flops 2048 | bytes 16384 | tf_op jit(solution)/shard_map/psum | solution.py:228
  221.1 6.4 %fusion.4 = bf16[1,2048,512]{2,1,0:T(8,128)(2,1)} fusion(bf16[1024,2048]{1,0:T(8,128)(2,1)} %all-gather.3.cloned.1.call-done, bf16[1024,512]{0,1:T(8,128)(2,1)} %copy-done.9), kind=kOutput, calls=%fused_computation.8 | convolution fusion | flops 2148532224 | bytes 7340032 | tf_op jit(solution)/shard_map/dot_general | solution.py:230
  231.2 3.8 %fusion.3 = bf16[1,512,2048]{2,1,0:T(8,128)(2,1)} fusion(bf16[1024,512]{0,1:T(8,128)(2,1)S(1)} %copy-done.10, bf16[1024,2048]{1,0:T(8,128)(2,1)S(1)} %copy-done.6, f32[1024]{0:T(1024)S(1)} %get-tuple-element.16), kind=kOutput, calls=%fused_computation.7 | convolution fusion | flops 2154823680 | bytes 7344128 | tf_op jit(solution)/shard_map/dot_general | solution.py:236
  235.0 53.0 %reduce-scatter.5.cloned.1.call-done = bf16[128,512]{1,0:T(8,128)(2,1)} async-done(((bf16[1024,512]{1,0:T(8,128)(2,1)}), bf16[128,512]{1,0:T(8,128)(2,1)}) %reduce-scatter.5.cloned.1.call-update) | async-done | bytes 131088 | tf_op jit(solution)/shard_map/reduce_scatter | solution.py:174
  (80 shorter events, 28.7 us)
Async XLA Ops:
  7.2 140.6 %copy-start = (bf16[1,2048,512]{2,1,0:T(8,128)(2,1)S(1)}, bf16[1,2048,512]{2,1,0:T(8,128)(2,1)}, u32[]{:S(2)}) copy-start(bf16[1,2048,512]{2,1,0:T(8,128)(2,1)} %param.13) | copy-start | bytes 6291460
  7.2 136.9 %all-gather.3.cloned.1.call-start = ((), (), s32[]{:S(2)}) async-start(), calls=%async_computation.2 | async-start | bytes 5242880 | tf_op jit(solution)/shard_map/all_gather | solution.py:169
  8.3 9.6 %collective-permute-start = (bf16[128,512]{1,0:T(8,128)(2,1)S(1)}, bf16[128,512]{1,0:T(8,128)(2,1)S(1)}, u32[]{:S(2)}, u32[]{:S(2)}) collective-permute-start(bf16[128,512]{1,0:T(8,128)(2,1)S(1)} %constant_dynamic-slice_fusion.3), channel_id=1, source_target_pairs={{0,4},{4,8},{8,12},{12,16},{16,20},{20,24},{24,28},{28,0},{1,5},{5... | collective-permute-start | bytes 393224 | tf_op jit(solution)/shard_map/ppermute | solution.py:165
  17.8 7.7 %collective-permute-start.1 = (bf16[128,512]{1,0:T(8,128)(2,1)S(1)}, bf16[128,512]{1,0:T(8,128)(2,1)S(1)}, u32[]{:S(2)}, u32[]{:S(2)}) collective-permute-start(bf16[128,512]{1,0:T(8,128)(2,1)S(1)} %collective-permute-done), channel_id=1, source_target_pairs={{0,4},{4,8},{8,12},{12,16},{16,20},{20,24},{24,28},{28,0},{1,5},{5... | collective-permute-start | bytes 393224 | tf_op jit(solution)/shard_map/ppermute | solution.py:165
  25.5 7.7 %collective-permute-start.2 = (bf16[128,512]{1,0:T(8,128)(2,1)S(1)}, bf16[128,512]{1,0:T(8,128)(2,1)S(1)}, u32[]{:S(2)}, u32[]{:S(2)}) collective-permute-start(bf16[128,512]{1,0:T(8,128)(2,1)S(1)} %collective-permute-done.1), channel_id=1, source_target_pairs={{0,4},{4,8},{8,12},{12,16},{16,20},{20,24},{24,28},{28,0},{1,5},{5... | collective-permute-start | bytes 393224 | tf_op jit(solution)/shard_map/ppermute | solution.py:165
  33.2 7.7 %collective-permute-start.3 = (bf16[128,512]{1,0:T(8,128)(2,1)S(1)}, bf16[128,512]{1,0:T(8,128)(2,1)S(1)}, u32[]{:S(2)}, u32[]{:S(2)}) collective-permute-start(bf16[128,512]{1,0:T(8,128)(2,1)S(1)} %collective-permute-done.2), channel_id=1, source_target_pairs={{0,4},{4,8},{8,12},{12,16},{16,20},{20,24},{24,28},{28,0},{1,5},{5... | collective-permute-start | bytes 393224 | tf_op jit(solution)/shard_map/ppermute | solution.py:165
  40.8 7.7 %collective-permute-start.4 = (bf16[128,512]{1,0:T(8,128)(2,1)S(1)}, bf16[128,512]{1,0:T(8,128)(2,1)S(1)}, u32[]{:S(2)}, u32[]{:S(2)}) collective-permute-start(bf16[128,512]{1,0:T(8,128)(2,1)S(1)} %collective-permute-done.3), channel_id=1, source_target_pairs={{0,4},{4,8},{8,12},{12,16},{16,20},{20,24},{24,28},{28,0},{1,5},{5... | collective-permute-start | bytes 393224 | tf_op jit(solution)/shard_map/ppermute | solution.py:165
  48.5 8.9 %collective-permute-start.5 = (bf16[128,512]{1,0:T(8,128)(2,1)S(1)}, bf16[128,512]{1,0:T(8,128)(2,1)S(1)}, u32[]{:S(2)}, u32[]{:S(2)}) collective-permute-start(bf16[128,512]{1,0:T(8,128)(2,1)S(1)} %collective-permute-done.4), channel_id=1, source_target_pairs={{0,4},{4,8},{8,12},{12,16},{16,20},{20,24},{24,28},{28,0},{1,5},{5... | collective-permute-start | bytes 393224 | tf_op jit(solution)/shard_map/ppermute | solution.py:165
  57.4 7.7 %collective-permute-start.6 = (bf16[128,512]{1,0:T(8,128)(2,1)S(1)}, bf16[128,512]{1,0:T(8,128)(2,1)S(1)}, u32[]{:S(2)}, u32[]{:S(2)}) collective-permute-start(bf16[128,512]{1,0:T(8,128)(2,1)S(1)} %collective-permute-done.5), channel_id=1, source_target_pairs={{0,4},{4,8},{8,12},{12,16},{16,20},{20,24},{24,28},{28,0},{1,5},{5... | collective-permute-start | bytes 393224 | tf_op jit(solution)/shard_map/ppermute | solution.py:165
  65.1 3.9 %copy-start.3 = (bf16[128,2048]{1,0:T(8,128)(2,1)S(1)}, bf16[128,2048]{1,0:T(8,128)(2,1)}, u32[]{:S(2)}) copy-start(bf16[128,2048]{1,0:T(8,128)(2,1)} %param.10) | copy-start | bytes 1572868
  69.0 90.8 %all-gather.5.cloned.1.call-start = ((), (), s32[]{:S(2)}) async-start(), calls=%async_computation.3 | async-start | bytes 5242880 | tf_op jit(solution)/shard_map/all_gather | solution.py:169
  69.1 7.7 %collective-permute-start.7 = (bf16[128,512]{1,0:T(8,128)(2,1)S(1)}, bf16[128,512]{1,0:T(8,128)(2,1)S(1)}, u32[]{:S(2)}, u32[]{:S(2)}) collective-permute-start(bf16[128,512]{1,0:T(8,128)(2,1)S(1)} %constant_dynamic-slice_fusion.2), channel_id=1, source_target_pairs={{0,4},{4,8},{8,12},{12,16},{16,20},{20,24},{24,28},{28,0},{1,5},{5... | collective-permute-start | bytes 393224 | tf_op jit(solution)/shard_map/ppermute | solution.py:165
  76.8 7.7 %collective-permute-start.8 = (bf16[128,512]{1,0:T(8,128)(2,1)S(1)}, bf16[128,512]{1,0:T(8,128)(2,1)S(1)}, u32[]{:S(2)}, u32[]{:S(2)}) collective-permute-start(bf16[128,512]{1,0:T(8,128)(2,1)S(1)} %collective-permute-done.7), channel_id=1, source_target_pairs={{0,4},{4,8},{8,12},{12,16},{16,20},{20,24},{24,28},{28,0},{1,5},{5... | collective-permute-start | bytes 393224 | tf_op jit(solution)/shard_map/ppermute | solution.py:165
  84.5 7.7 %collective-permute-start.9 = (bf16[128,512]{1,0:T(8,128)(2,1)S(1)}, bf16[128,512]{1,0:T(8,128)(2,1)S(1)}, u32[]{:S(2)}, u32[]{:S(2)}) collective-permute-start(bf16[128,512]{1,0:T(8,128)(2,1)S(1)} %collective-permute-done.8), channel_id=1, source_target_pairs={{0,4},{4,8},{8,12},{12,16},{16,20},{20,24},{24,28},{28,0},{1,5},{5... | collective-permute-start | bytes 393224 | tf_op jit(solution)/shard_map/ppermute | solution.py:165
  92.1 8.0 %collective-permute-start.10 = (bf16[128,512]{1,0:T(8,128)(2,1)S(1)}, bf16[128,512]{1,0:T(8,128)(2,1)S(1)}, u32[]{:S(2)}, u32[]{:S(2)}) collective-permute-start(bf16[128,512]{1,0:T(8,128)(2,1)S(1)} %collective-permute-done.9), channel_id=1, source_target_pairs={{0,4},{4,8},{8,12},{12,16},{16,20},{20,24},{24,28},{28,0},{1,5},{5... | collective-permute-start | bytes 393224 | tf_op jit(solution)/shard_map/ppermute | solution.py:165
  100.2 9.0 %collective-permute-start.11 = (bf16[128,512]{1,0:T(8,128)(2,1)S(1)}, bf16[128,512]{1,0:T(8,128)(2,1)S(1)}, u32[]{:S(2)}, u32[]{:S(2)}) collective-permute-start(bf16[128,512]{1,0:T(8,128)(2,1)S(1)} %collective-permute-done.10), channel_id=1, source_target_pairs={{0,4},{4,8},{8,12},{12,16},{16,20},{20,24},{24,28},{28,0},{1,5},{5... | collective-permute-start | bytes 393224 | tf_op jit(solution)/shard_map/ppermute | solution.py:165
  109.1 7.7 %collective-permute-start.12 = (bf16[128,512]{1,0:T(8,128)(2,1)S(1)}, bf16[128,512]{1,0:T(8,128)(2,1)S(1)}, u32[]{:S(2)}, u32[]{:S(2)}) collective-permute-start(bf16[128,512]{1,0:T(8,128)(2,1)S(1)} %collective-permute-done.11), channel_id=1, source_target_pairs={{0,4},{4,8},{8,12},{12,16},{16,20},{20,24},{24,28},{28,0},{1,5},{5... | collective-permute-start | bytes 393224 | tf_op jit(solution)/shard_map/ppermute | solution.py:165
  116.8 7.7 %collective-permute-start.13 = (bf16[128,512]{1,0:T(8,128)(2,1)S(1)}, bf16[128,512]{1,0:T(8,128)(2,1)S(1)}, u32[]{:S(2)}, u32[]{:S(2)}) collective-permute-start(bf16[128,512]{1,0:T(8,128)(2,1)S(1)} %collective-permute-done.12), channel_id=1, source_target_pairs={{0,4},{4,8},{8,12},{12,16},{16,20},{20,24},{24,28},{28,0},{1,5},{5... | collective-permute-start | bytes 393224 | tf_op jit(solution)/shard_map/ppermute | solution.py:165
  124.6 19.5 %copy-start.4 = (bf16[2048,4]{0,1:T(4,128)(2,1)S(1)}, bf16[2048,4]{0,1:T(4,128)(2,1)}, u32[]{:S(2)}) copy-start(bf16[2048,4]{0,1:T(4,128)(2,1)} %param.12) | copy-start | bytes 49156
  127.5 93.0 %reduce-scatter.3.cloned.1.call-start = ((), (), s32[]{:S(2)}) async-start(), calls=%async_computation.4 | async-start | bytes 5242880 | tf_op jit(solution)/shard_map/reduce_scatter | solution.py:173
  147.8 3.8 %copy-start.7 = (bf16[1,2048,512]{2,1,0:T(8,128)(2,1)S(1)}, bf16[1,2048,512]{2,1,0:T(8,128)(2,1)}, u32[]{:S(2)}) copy-start(bf16[1,2048,512]{2,1,0:T(8,128)(2,1)} %param.14) | copy-start | bytes 6291460
  175.2 112.7 %reduce-scatter.5.cloned.1.call-start = ((), (), s32[]{:S(2)}) async-start(), calls=%async_computation.5 | async-start | bytes 1179648 | tf_op jit(solution)/shard_map/reduce_scatter | solution.py:174
  221.1 6.4 %copy-start.2 = (bf16[1024,2048]{1,0:T(8,128)(2,1)S(1)}, bf16[1024,2048]{1,0:T(8,128)(2,1)}, u32[]{:S(2)}) copy-start(bf16[1024,2048]{1,0:T(8,128)(2,1)} %all-gather.3.cloned.1.call-done) | copy-start | bytes 12582916
  227.5 3.7 %copy-start.10 = (bf16[1024,512]{0,1:T(8,128)(2,1)S(1)}, bf16[1024,512]{0,1:T(8,128)(2,1)}, u32[]{:S(2)}) copy-start(bf16[1024,512]{0,1:T(8,128)(2,1)} %get-tuple-element.10) | copy-start | bytes 3145732
  (5 other events, 15.2 us)
Sparse Core Ops, SparseCore 0:
  69.1 32.1 all-gather.2
  127.6 32.1 all-gather.4
  175.3 45.1 reduce-scatter.2
  223.7 64.1 reduce-scatter.4
